TPU v7x, 256 devices: a whole 4x4x8 slice. The times are simulated.
256 devices in a mesh: sp: 64 (over z, y, core), tp: 4 (over x).
Axes of the slice: x: 4, y: 4, z: 8, core: 2. Of those that a mesh axis runs over, the one named last changes fastest.
Arguments:
- residual: bfloat16 [65536, 2048], P(('sp', 'tp')), may hold values from -6 to 6
- pool_input: bfloat16 [65536, 1024], P('sp', 'tp'), may hold values from -6 to 6
- doc_ids: int32 [65536], P('sp'), may hold values from 0 to 31, never falling along the last dimension, each value on 1 to 4096 neighbouring positions
- pool_map: bfloat16 [4, 256, 256], P('tp'), may hold values from -0.375 to 0.375
- pool_scale: float32 [1024], P('tp'), may hold values from 0.1 to 1.9
- out_weight: bfloat16 [1024, 2048], replicated, may hold values from -0.1875 to 0.1875
- mix_gain: float32 [2048], replicated, may hold values from 0.1 to 1.9
- mix_shift: float32 [2048], replicated, may hold values from -1.75 to 1.75
- group_router: bfloat16 [2048, 4], replicated, may hold values from -0.125 to 0.125
- expert_router: bfloat16 [2048, 64], replicated, may hold values from -0.125 to 0.125
- expert_gate: bfloat16 [64, 2048, 512], P('sp'), may hold values from -0.375 to 0.375
- expert_up: bfloat16 [64, 2048, 512], P('sp'), may hold values from -0.375 to 0.375
- expert_down: bfloat16 [64, 512, 2048], P('sp'), may hold values from -0.75 to 0.75
- routes: int32 [65536, 2], P(('sp', 'tp')), may hold values from 0 to 63, as said below
- ffn_gain: float32 [2048], replicated, may hold values from 0.1 to 1.9
- ffn_shift: float32 [2048], replicated, may hold values from -1.75 to 1.75
Outputs:
- layer_out: bfloat16 [65536, 2048], P(('sp', 'tp'))
Inputs may be any that keep to these rules, and one draw needn't show every extreme that they name: `doc_ids`: document numbers never fall along the positions; each document has 1 to 4096 positions. `routes`: A token names 2 different experts. In each aligned block of half of one device's 256 rows, 32 experts are named exactly 8 times each and the others not at all.
All inputs are finite; a program needn't handle non-finite values.
Results may differ from a plain program's by a relative error of at most 0.0073.
Values may be sent and summed in bfloat16 or wider, within the bound.
No kernel may reach another device: no remote copies, remote signals or barrier semaphores. Data moves between devices by JAX's collectives and lax.ppermute only.
A program may use at most 128 MiB of HBM per device.

v0:
```python
import functools

import jax
import jax.numpy as jnp
from jax import lax
from jax.experimental import pallas as pl
from jax.experimental.pallas import tpu as pltpu
from jax.sharding import PartitionSpec as P

skip_scale = 2.0**0.5
epsilon = 1e-05
f32 = jnp.float32
bf16 = jnp.bfloat16

TAIL = 16
BLK = 128
CHANNELS = 256
HALF = 128
SLOTS = 512
EXPERTS = 64
WIDTH = 2048
CHUNKS = 4


VMEM = pl.BlockSpec(memory_space=pltpu.VMEM)
HBM = pl.BlockSpec(memory_space=pltpu.MemorySpace.HBM)
ROOM = pltpu.CompilerParams(vmem_limit_bytes=48 * 2**20)


def in_hbm(*arrays):
    held = [pltpu.with_memory_space_constraint(a, pltpu.MemorySpace.HBM) for a in arrays]
    return held if len(held) > 1 else held[0]


def dot(a, b, dims=((1,), (0,)), **kw):
    return lax.dot_general(a, b, (dims, ((), ())), preferred_element_type=f32, **kw)


def pool_kernel(half, *refs):
    if half == 0:
        tail, refs = refs[0], refs[1:]
    x, docs_in, map_in, scale_in, out0, out1, out2, out3 = refs[:8]
    xs, ds, docs, pool_map, scale, sems = refs[-6:]
    tp, sp = lax.axis_index("tp"), lax.axis_index("sp")
    loads = [
        pltpu.make_async_copy(docs_in, docs, sems.at[0]),
        pltpu.make_async_copy(x, xs.at[pl.ds(BLK, x.shape[0]), :], sems.at[1]),
        pltpu.make_async_copy(map_in, pool_map, sems.at[2]),
        pltpu.make_async_copy(scale_in, scale, sems.at[3]),
    ]
    for load in loads:
        load.start()
    if half == 0:
        xs[0 : BLK - TAIL, :] = jnp.zeros((BLK - TAIL, CHANNELS), bf16)
        xs[BLK - TAIL : BLK, :] = tail[0:TAIL, :]
        tail_docs = tail[TAIL : TAIL + 1, 0:BLK].astype(f32)
        ds[0:1, :] = jnp.where(sp == 0, -1.0, tail_docs)
    loads[0].wait()
    ds[1:9, :] = docs[...].astype(f32)
    window = jnp.left_shift(jnp.int32(2), tp)
    t_pos = lax.broadcasted_iota(jnp.int32, (BLK, BLK), 0)
    s_pos = lax.broadcasted_iota(jnp.int32, (BLK, BLK), 1)
    back = t_pos - s_pos
    in_cur = (back >= 0) & (back < window)
    in_prev = back + BLK < window
    kept = []
    for d in range(4):
        b = ((tp + d) % 4) * 2 + half
        prev_docs = ds[pl.ds(b, 1), :]
        cur_docs = ds[pl.ds(b + 1, 1), :]
        own_docs = jnp.transpose(jnp.broadcast_to(cur_docs, (BLK, BLK)))
        keep_cur = jnp.where(in_cur & (own_docs == cur_docs), 1.0, 0.0)
        keep_prev = jnp.where(in_prev & (own_docs == prev_docs), 1.0, 0.0)
        count = jnp.sum(keep_cur + keep_prev, axis=1, keepdims=True)
        kept.append((b, keep_cur.astype(bf16), keep_prev.astype(bf16), count))
    for load in loads[1:]:
        load.wait()
    group = pool_map[0]
    for (b, keep_cur, keep_prev, count), out in zip(kept, (out0, out1, out2, out3)):
        row = pl.multiple_of(b * BLK, BLK)
        cur = xs[pl.ds(row + BLK, BLK), :]
        prev = xs[pl.ds(row, BLK), :]
        running = dot(keep_cur, cur) + dot(keep_prev, prev)
        pooled = (running / count - cur.astype(f32)).astype(bf16)
        mixed = dot(pooled, group) * scale[...]
        out[...] = mixed.astype(bf16)
    if half == 1:
        message = refs[8]
        message[0:TAIL, :] = xs[BLK + x.shape[0] - TAIL :, :]
        message[TAIL:, 0:BLK] = jnp.broadcast_to(ds[8:9, :], (TAIL, BLK)).astype(bf16)
        message[TAIL:, BLK:] = jnp.zeros((TAIL, CHANNELS - BLK), bf16)


def pool(half, x, docs, pool_map, scale, tail=None):
    rows = x.shape[0]
    shapes = [jax.ShapeDtypeStruct((HALF, CHANNELS), bf16)] * 4
    if half == 1:
        shapes.append(jax.ShapeDtypeStruct((2 * TAIL, CHANNELS), bf16))
    first = [] if tail is None else [tail]
    return pl.pallas_call(
        functools.partial(pool_kernel, half),
        out_shape=shapes,
        in_specs=[VMEM] * len(first) + [HBM] * 4,
        out_specs=[VMEM] * len(shapes),
        scratch_shapes=[
            pltpu.VMEM((rows + BLK, CHANNELS), bf16),
            pltpu.VMEM((16, BLK), f32),
            pltpu.VMEM(docs.shape, jnp.int32),
            pltpu.VMEM(pool_map.shape, bf16),
            pltpu.VMEM(scale.shape, f32),
            pltpu.SemaphoreType.DMA((4,)),
        ],
        name="pool",
        compiler_params=ROOM,
    )(*first, *in_hbm(x, docs, pool_map, scale))


def slots_of(chosen):
    strict = (
        lax.broadcasted_iota(jnp.int32, (HALF, HALF), 1)
        < lax.broadcasted_iota(jnp.int32, (HALF, HALF), 0)
    )
    strict = jnp.where(strict, 1.0, 0.0).astype(bf16)
    expert = lax.broadcasted_iota(jnp.int32, (HALF, EXPERTS), 1)
    slot = lax.broadcasted_iota(jnp.int32, (HALF, SLOTS), 1)
    first, second = chosen[:, 0:1], chosen[:, 1:2]
    hot0 = jnp.where(expert == first, 1.0, 0.0)
    hot1 = jnp.where(expert == second, 1.0, 0.0)
    before0 = dot(strict, hot0.astype(bf16))
    before1 = dot(strict, hot1.astype(bf16)) + jnp.sum(hot0, axis=0, keepdims=True)
    rank0 = jnp.sum(before0 * hot0, axis=1, keepdims=True).astype(jnp.int32)
    rank1 = jnp.sum(before1 * hot1, axis=1, keepdims=True).astype(jnp.int32)
    return slot == first * 8 + rank0, slot == second * 8 + rank1


def slot_kernel(routes, weight, gather, near_weight, sem):
    load = pltpu.make_async_copy(weight, near_weight, sem)
    load.start()
    for h in range(2):
        hit0, hit1 = slots_of(routes[h * HALF : (h + 1) * HALF, :])
        hit = jnp.where(hit0 | hit1, 1.0, 0.0)
        gather[h] = jnp.transpose(hit).astype(bf16)
    load.wait()


def slots(routes, weight):
    return pl.pallas_call(
        slot_kernel,
        out_shape=[
            jax.ShapeDtypeStruct((2, SLOTS, HALF), bf16),
            jax.ShapeDtypeStruct(weight.shape, bf16),
        ],
        in_specs=[VMEM, HBM],
        out_specs=[VMEM] * 2,
        scratch_shapes=[pltpu.SemaphoreType.DMA],
        name="slots",
        compiler_params=ROOM,
    )(routes, weight)


def norm(values, gain, shift):
    mean = jnp.mean(values, axis=-1, keepdims=True)
    center = values - mean
    var = jnp.mean(center * center, axis=-1, keepdims=True)
    return center * lax.rsqrt(var + epsilon) * gain + shift


def mix_kernel(
    half, m0, m1, m2, m3, weight, residual, gain, shift, gather, rows_out, res, rows, sems
):
    tp = lax.axis_index("tp")
    load = pltpu.make_async_copy(residual.at[pl.ds(half * HALF, HALF), :], res, sems.at[CHUNKS])
    load.start()
    branch = None
    for d, m in enumerate((m0, m1, m2, m3)):
        group = (tp + 4 - d) % 4
        row = pl.multiple_of(group * CHANNELS, CHANNELS)
        term = dot(m[...], weight[pl.ds(row, CHANNELS), :])
        branch = term if branch is None else branch + term
    load.wait()
    values = skip_scale * res[...].astype(f32) + branch
    normed = norm(values, gain[...], shift[...]).astype(bf16)
    stores = []
    for c in range(CHUNKS):
        part = slice(c * SLOTS // CHUNKS, (c + 1) * SLOTS // CHUNKS)
        rows[part, :] = dot(gather[half, part, :], normed).astype(bf16)
        stores.append(pltpu.make_async_copy(rows.at[part, :], rows_out.at[part, :], sems.at[c]))
        stores[-1].start()
    for store in stores:
        store.wait()


def mix(half, parts, weight, residual, gain, shift, gather):
    return pl.pallas_call(
        functools.partial(mix_kernel, half),
        out_shape=jax.ShapeDtypeStruct((SLOTS, WIDTH), bf16),
        in_specs=[VMEM] * 5 + [HBM] + [VMEM] * 3,
        out_specs=HBM,
        scratch_shapes=[
            pltpu.VMEM((HALF, WIDTH), bf16),
            pltpu.VMEM((SLOTS, WIDTH), bf16),
            pltpu.SemaphoreType.DMA((CHUNKS + 1,)),
        ],
        name="mix",
        compiler_params=ROOM,
    )(*parts, weight, in_hbm(residual), gain, shift, gather)


def weight_kernel(half, laid_out, group_router, expert_router, routes, normed, split):
    hit0, hit1 = slots_of(routes[half * HALF : (half + 1) * HALF, :])
    rows = dot(jnp.where(hit0, 1.0, 0.0).astype(bf16), laid_out[...]).astype(bf16)
    normed[...] = rows
    group_logits = dot(rows, group_router[...])
    expert_logits = dot(rows, expert_router[...])
    group_exp = jnp.exp(group_logits)
    group_prob = group_exp / jnp.sum(group_exp, axis=1, keepdims=True)
    slot = lax.broadcasted_iota(jnp.int32, (EXPERTS, SLOTS), 1)
    expert = lax.broadcasted_iota(jnp.int32, (EXPERTS, SLOTS), 0)
    widen = jnp.where(slot // 8 == expert, 1.0, 0.0)
    slot = lax.broadcasted_iota(jnp.int32, (4, SLOTS), 1)
    group = lax.broadcasted_iota(jnp.int32, (4, SLOTS), 0)
    widen_group = jnp.where(slot // (SLOTS // 4) == group, 1.0, 0.0)
    logits = dot(expert_logits, widen, precision=lax.Precision.HIGHEST)
    share = dot(group_prob, widen_group, precision=lax.Precision.HIGHEST)
    hit = hit0 | hit1
    picked_exp = jnp.where(hit, jnp.exp(logits), 0.0)
    pair_share = picked_exp / jnp.sum(picked_exp, axis=1, keepdims=True)
    weight = jnp.where(hit, share * pair_share, 0.0)
    high = weight.astype(bf16)
    split[0:HALF, :] = high
    split[HALF:, :] = (weight - high.astype(f32)).astype(bf16)


def weights(half, laid_out, group_router, expert_router, routes):
    return pl.pallas_call(
        functools.partial(weight_kernel, half),
        out_shape=[
            jax.ShapeDtypeStruct((HALF, WIDTH), bf16),
            jax.ShapeDtypeStruct((2 * HALF, SLOTS), bf16),
        ],
        in_specs=[VMEM] * 4,
        out_specs=[VMEM] * 2,
        name="weights",
    )(laid_out, group_router, expert_router, routes)


def finish_kernel(split, returned, normed, gain, shift, *rest):
    out = rest[-1]
    both = dot(split[...], returned[...])
    routed = both[0:HALF, :] + both[HALF:, :]
    values = skip_scale * normed[...].astype(f32) + routed
    out[...] = norm(values, gain[...], shift[...]).astype(bf16)


def finish(half, split, returned, normed, gain, shift, base=None):
    def full(*shape):
        return pl.BlockSpec(shape, lambda i: (0,) * len(shape))

    operands = [split, returned, normed, gain, shift]
    in_specs = [full(*a.shape) for a in operands]
    aliases = {}
    if base is not None:
        operands.append(base)
        in_specs.append(HBM)
        aliases = {5: 0}
    return pl.pallas_call(
        finish_kernel,
        grid=(1,),
        out_shape=jax.ShapeDtypeStruct((2 * HALF, WIDTH), bf16),
        in_specs=in_specs,
        out_specs=pl.BlockSpec((HALF, WIDTH), lambda i: (half, 0)),
        input_output_aliases=aliases,
        name="finish",
    )(*operands)


def expert_ffn(arrived, expert_gate, expert_up, expert_down):
    gate_out = jnp.dot(arrived, expert_gate[0], preferred_element_type=f32)
    up_out = jnp.dot(arrived, expert_up[0], preferred_element_type=f32)
    hidden = (jax.nn.silu(gate_out) * up_out).astype(bf16)
    return jnp.dot(hidden, expert_down[0], preferred_element_type=f32).astype(bf16)


def exchange(rows):
    blocks = rows.reshape(EXPERTS, SLOTS // EXPERTS, WIDTH)
    moved = lax.all_to_all(blocks, "sp", split_axis=0, concat_axis=0, tiled=True)
    return moved.reshape(SLOTS, WIDTH)


def on_device(
    residual,
    pool_input,
    doc_ids,
    pool_map,
    pool_scale,
    out_weight,
    mix_gain,
    mix_shift,
    group_router,
    expert_router,
    expert_gate,
    expert_up,
    expert_down,
    routes,
    ffn_gain,
    ffn_shift,
):
    sp_count = lax.axis_size("sp")
    docs = doc_ids.reshape(doc_ids.shape[0] // BLK, BLK)
    inputs = (pool_input, docs, pool_map, pool_scale[None, :])
    parts, tail = {}, None
    for h in (1, 0):
        blocks = pool(h, *inputs, tail=tail)
        parts[h] = [blocks[0]] + [
            lax.ppermute(blocks[d], "tp", [(i, (i + d) % 4) for i in range(4)])
            for d in range(1, 4)
        ]
        if h == 1:
            tail = lax.ppermute(blocks[4], "sp", [(i, i + 1) for i in range(sp_count - 1)])
            gather, near_weight = slots(routes, out_weight)
            near_weight = pltpu.with_memory_space_constraint(near_weight, pltpu.VMEM)
    arrived, kept = {}, {}
    for h in (1, 0):
        outgoing = mix(
            h,
            parts[h],
            (out_weight, near_weight)[h],
            residual,
            mix_gain[None, :],
            mix_shift[None, :],
            gather,
        )
        arrived[h] = exchange(outgoing)
        kept[h] = weights(h, outgoing, group_router, expert_router, routes)
    result = None
    for h in (1, 0):
        returned = exchange(expert_ffn(arrived[h], expert_gate, expert_up, expert_down))
        normed, split = kept[h]
        result = finish(
            h, split, returned, normed, ffn_gain[None, :], ffn_shift[None, :], result
        )
    return result


def solution(mesh):
    in_specs = (
        P(("sp", "tp"), None),
        P("sp", "tp"),
        P("sp"),
        P("tp", None, None),
        P("tp"),
        P(),
        P(),
        P(),
        P(),
        P(),
        P("sp", None, None),
        P("sp", None, None),
        P("sp", None, None),
        P(("sp", "tp"), None),
        P(),
        P(),
    )
    out_specs = P(("sp", "tp"), None)
    return jax.shard_map(
        on_device, mesh=mesh, in_specs=in_specs, out_specs=out_specs, check_vma=False
    )
```

profile of v0, /device:TPU:8, one launch (start us, length us, event | category | flops | bytes accessed | tf_op | source)
XLA Modules:
  0.0 267.5 jit_solution(3072780751928836832)
XLA Ops:
  0.0 0.0 copy-start
  0.0 2.2 pool.2
  2.2 1.6 collective-permute-start.4
  3.7 2.7 %collective-permute-start.5 = (bf16[128,256]{1,0:T(8,128)(2,1)S(1)}, bf16[128,256]{1,0:T(8,128)(2,1)S(1)}, u32[]{:S(2)}, u32[]{:S(2)}) collective-permute-start(bf16[128,256]{1,0:T(8,128)(2,1)S(1)} %get-tuple-element.30), channel_id=1, source_target_pairs={{0,2},{1,3},{2,0},{3,1},{4,6},{5,7},{6,4},{7,5},{8,10},{9,11},{10,... | collective-permute-start | bytes 196616 | tf_op jit(solution)/shard_map/ppermute | solution.py:315
  6.5 1.4 collective-permute-start.6
  7.9 0.8 copy.18.routes
  8.7 0.0 copy-start.2
  8.7 0.0 copy-start.3
  8.7 0.0 copy-start.4
  8.8 2.3 slots.1
  11.0 0.0 copy-done.2
  11.0 0.0 collective-permute-done.4.m1
  11.0 0.0 collective-permute-done.5.m2
  11.0 0.0 collective-permute-done.6.m3
  11.1 0.0 copy-done.3
  11.1 0.0 copy-done.4
  11.1 3.7 %mix.3.laid_out = bf16[512,2048]{1,0:T(8,128)(2,1)} custom-call(bf16[128,256]{1,0:T(8,128)(2,1)S(1)} %get-tuple-element.28.m0, bf16[128,256]{1,0:T(8,128)(2,1)S(1)} %collective-permute-done.4.m1, bf16[128,256]{1,0:T(8,128)(2,1)S(1)} %collective-permute-done.5.m2, bf16[128,256]{1,0:T(8,128)(2,1)S(1)} %collective-permute-done.6.m3, ...), custom_call_target="tpu_custom_call" | custom-call | tf_op jit(solution)/shard_map/mix/pallas_call | solution.py:194
  14.8 12.3 %all-to-all-start.2 = ((bf16[64,8,2048]{2,1,0:T(8,128)(2,1)}), bf16[64,8,2048]{2,1,0:T(8,128)(2,1)}, u32[]{:S(2)}, u32[]{:S(2)}) async-start(bf16[64,8,2048]{2,1,0:T(8,128)(2,1)} %bitcast.60), calls=%async_computation.2 | async-start | bytes 4194304 | tf_op jit(solution)/shard_map/all_to_all | solution.py:286
  27.1 2.0 collective-permute-start
  29.1 4.0 %collective-permute-done.refs_0_ = bf16[32,256]{1,0:T(8,128)(2,1)S(1)} collective-permute-done((bf16[32,256]{1,0:T(8,128)(2,1)S(1)}, bf16[32,256]{1,0:T(8,128)(2,1)S(1)}, u32[]{:S(2)}, u32[]{:S(2)}) %collective-permute-start) | collective-permute-done | bytes 16416 | tf_op jit(solution)/shard_map/ppermute | solution.py:319
  33.1 2.0 pool.3
  35.1 0.7 collective-permute-start.1
  35.8 3.2 %collective-permute-start.2 = (bf16[128,256]{1,0:T(8,128)(2,1)S(1)}, bf16[128,256]{1,0:T(8,128)(2,1)S(1)}, u32[]{:S(2)}, u32[]{:S(2)}) collective-permute-start(bf16[128,256]{1,0:T(8,128)(2,1)S(1)} %get-tuple-element.23), channel_id=1, source_target_pairs={{0,2},{1,3},{2,0},{3,1},{4,6},{5,7},{6,4},{7,5},{8,10},{9,11},{10,... | collective-permute-start | bytes 196616 | tf_op jit(solution)/shard_map/ppermute | solution.py:315
  39.0 0.1 collective-permute-start.3
  39.1 1.8 collective-permute-done.1.m1
  40.9 1.0 collective-permute-done.2.m2
  41.9 1.3 collective-permute-done.3.m3
  43.2 5.5 %mix.2.laid_out = bf16[512,2048]{1,0:T(8,128)(2,1)S(1)} custom-call(bf16[128,256]{1,0:T(8,128)(2,1)S(1)} %get-tuple-element.21.m0, bf16[128,256]{1,0:T(8,128)(2,1)S(1)} %collective-permute-done.1.m1, bf16[128,256]{1,0:T(8,128)(2,1)S(1)} %collective-permute-done.2.m2, bf16[128,256]{1,0:T(8,128)(2,1)S(1)} %collective-permute-done.3.m3, ...), custom_call_target="tpu_custom_call" | custom-call | tf_op jit(solution)/shard_map/mix/pallas_call | solution.py:194
  48.7 0.0 copy-start.1
  48.7 1.3 copy-done.1
  50.1 28.2 %all-to-all-done.2 = bf16[64,8,2048]{2,1,0:T(8,128)(2,1)} async-done(((bf16[64,8,2048]{2,1,0:T(8,128)(2,1)}), bf16[64,8,2048]{2,1,0:T(8,128)(2,1)}, u32[]{:S(2)}, u32[]{:S(2)}) %all-to-all-start.2) | async-done | bytes 2097184 | tf_op jit(solution)/shard_map/all_to_all | solution.py:286
  78.3 20.9 %all-to-all-start = ((bf16[64,8,2048]{2,1,0:T(8,128)(2,1)}), bf16[64,8,2048]{2,1,0:T(8,128)(2,1)}, u32[]{:S(2)}, u32[]{:S(2)}) async-start(bf16[64,8,2048]{2,1,0:T(8,128)(2,1)} %bitcast.55), calls=%async_computation | async-start | bytes 4194304 | tf_op jit(solution)/shard_map/all_to_all | solution.py:286
  99.2 3.5 %fusion.2 = f32[512,512]{1,0:T(8,128)S(1)} fusion(bf16[64,8,2048]{2,1,0:T(8,128)(2,1)} %all-to-all-done.2, bf16[1,2048,512]{2,1,0:T(8,128)(2,1)} %param.27), kind=kOutput, calls=%fused_computation.4 | convolution fusion | flops 1073741824 | bytes 5242880 | tf_op jit(solution)/shard_map/dot_general | solution.py:279
  102.7 0.0 copy-done
  102.7 6.1 %fusion.1 = bf16[64,8,2048]{2,1,0:T(8,128)(2,1)} fusion(bf16[1,512,2048]{2,1,0:T(8,128)(2,1)S(1)} %copy-done, f32[512,512]{1,0:T(8,128)S(1)} %fusion.2, bf16[64,8,2048]{2,1,0:T(8,128)(2,1)} %all-to-all-done.2, bf16[1,2048,512]{2,1,0:T(8,128)(2,1)} %param.26), kind=kOutput, calls=%fused_computation.3 | convolution fusion | flops 2150105088 | bytes 9437184 | tf_op jit(solution)/shard_map/dot_general | solution.py:281
  108.7 41.6 %all-to-all-done = bf16[64,8,2048]{2,1,0:T(8,128)(2,1)} async-done(((bf16[64,8,2048]{2,1,0:T(8,128)(2,1)}), bf16[64,8,2048]{2,1,0:T(8,128)(2,1)}, u32[]{:S(2)}, u32[]{:S(2)}) %all-to-all-start) | async-done | bytes 2097184 | tf_op jit(solution)/shard_map/all_to_all | solution.py:286
  150.3 5.6 %all-to-all-start.3 = ((bf16[64,8,2048]{2,1,0:T(8,128)(2,1)}), bf16[64,8,2048]{2,1,0:T(8,128)(2,1)}, u32[]{:S(2)}, u32[]{:S(2)}) async-start(bf16[64,8,2048]{2,1,0:T(8,128)(2,1)} %fusion.1), calls=%async_computation.3 | async-start | bytes 4194304 | tf_op jit(solution)/shard_map/all_to_all | solution.py:286
  156.0 3.5 %fusion.9 = f32[512,512]{1,0:T(8,128)S(1)} fusion(bf16[1,2048,512]{2,1,0:T(8,128)(2,1)} %param.27, bf16[64,8,2048]{2,1,0:T(8,128)(2,1)} %all-to-all-done), kind=kOutput, calls=%fused_computation.11 | convolution fusion | flops 1073741824 | bytes 5242880 | tf_op jit(solution)/shard_map/dot_general | solution.py:279
  159.4 6.0 %fusion = bf16[64,8,2048]{2,1,0:T(8,128)(2,1)} fusion(bf16[1,512,2048]{2,1,0:T(8,128)(2,1)S(1)} %copy-done, f32[512,512]{1,0:T(8,128)S(1)} %fusion.9, bf16[1,2048,512]{2,1,0:T(8,128)(2,1)} %param.26, bf16[64,8,2048]{2,1,0:T(8,128)(2,1)} %all-to-all-done), kind=kOutput, calls=%fused_computation.2 | convolution fusion | flops 2150105088 | bytes 9437184 | tf_op jit(solution)/shard_map/dot_general | solution.py:281
  165.4 0.0 copy-start.6
  165.4 0.0 copy-start.5
  165.5 41.7 %all-to-all-done.3 = bf16[64,8,2048]{2,1,0:T(8,128)(2,1)} async-done(((bf16[64,8,2048]{2,1,0:T(8,128)(2,1)}), bf16[64,8,2048]{2,1,0:T(8,128)(2,1)}, u32[]{:S(2)}, u32[]{:S(2)}) %all-to-all-start.3) | async-done | bytes 2097184 | tf_op jit(solution)/shard_map/all_to_all | solution.py:286
  207.1 5.6 %all-to-all-start.1 = ((bf16[64,8,2048]{2,1,0:T(8,128)(2,1)}), bf16[64,8,2048]{2,1,0:T(8,128)(2,1)}, u32[]{:S(2)}, u32[]{:S(2)}) async-start(bf16[64,8,2048]{2,1,0:T(8,128)(2,1)} %fusion), calls=%async_computation.1 | async-start | bytes 4194304 | tf_op jit(solution)/shard_map/all_to_all | solution.py:286
  212.7 0.0 copy-done.6
  212.8 1.1 copy.19.group_router
  213.8 0.0 copy-done.5
  213.8 1.0 copy.20.expert_router
  214.8 4.2 %weights.3 = (bf16[128,2048]{1,0:T(8,128)(2,1)}, bf16[256,512]{1,0:T(8,128)(2,1)}) custom-call(bf16[512,2048]{1,0:T(8,128)(2,1)} %mix.3.laid_out, bf16[2048,4]{1,0:T(8,128)(2,1)} %copy.19.group_router, bf16[2048,64]{1,0:T(8,128)(2,1)} %copy.20.expert_router, s32[256,2]{1,0:T(8,128)} %copy-done.2), custom_call_target="tpu_custom_call" | custom-call | tf_op jit(solution)/shard_map/weights/pallas_call | solution.py:235
  219.0 4.2 %weights.2 = (bf16[128,2048]{1,0:T(8,128)(2,1)}, bf16[256,512]{1,0:T(8,128)(2,1)}) custom-call(bf16[512,2048]{1,0:T(8,128)(2,1)} %copy-done.1, bf16[2048,4]{1,0:T(8,128)(2,1)} %copy.19.group_router, bf16[2048,64]{1,0:T(8,128)(2,1)} %copy.20.expert_router, s32[256,2]{1,0:T(8,128)} %copy-done.2), custom_call_target="tpu_custom_call" | custom-call | tf_op jit(solution)/shard_map/weights/pallas_call | solution.py:235
  223.2 3.6 %finish.2.rest_0_ = bf16[256,2048]{1,0:T(8,128)(2,1)} custom-call(bf16[256,512]{1,0:T(8,128)(2,1)} %get-tuple-element.33.split, bf16[512,2048]{1,0:T(8,128)(2,1)} %bitcast.16.returned, bf16[128,2048]{1,0:T(8,128)(2,1)} %get-tuple-element.34.normed, f32[1,2048]{1,0:T(1,128)} %bitcast.61, f32[1,2048]{1,0:T(1,128)} %bitcast.63), custom_call_target="tpu_custom_call" | custom-call | tf_op jit(solution)/shard_map/finish/pallas_call | solution.py:266
  226.8 37.1 %all-to-all-done.1 = bf16[64,8,2048]{2,1,0:T(8,128)(2,1)} async-done(((bf16[64,8,2048]{2,1,0:T(8,128)(2,1)}), bf16[64,8,2048]{2,1,0:T(8,128)(2,1)}, u32[]{:S(2)}, u32[]{:S(2)}) %all-to-all-start.1) | async-done | bytes 2097184 | tf_op jit(solution)/shard_map/all_to_all | solution.py:286
  263.9 3.6 %finish.3 = bf16[256,2048]{1,0:T(8,128)(2,1)} custom-call(bf16[256,512]{1,0:T(8,128)(2,1)} %get-tuple-element.26.split, bf16[512,2048]{1,0:T(8,128)(2,1)} %bitcast.10.returned, bf16[128,2048]{1,0:T(8,128)(2,1)} %get-tuple-element.27.normed, f32[1,2048]{1,0:T(1,128)} %bitcast.62, f32[1,2048]{1,0:T(1,128)} %bitcast.64, ...), custom_call_target="tpu_custom_call", output_to_operand_aliasing={{}: (5, {})} | custom-call | tf_op jit(solution)/shard_map/finish/pallas_call | solution.py:266
Async XLA Ops:
  0.0 102.7 %copy-start = (bf16[1,512,2048]{2,1,0:T(8,128)(2,1)S(1)}, bf16[1,512,2048]{2,1,0:T(8,128)(2,1)}, u32[]{:S(2)}) copy-start(bf16[1,512,2048]{2,1,0:T(8,128)(2,1)} %param.28) | copy-start | bytes 6291460
  2.2 8.9 %collective-permute-start.4 = (bf16[128,256]{1,0:T(8,128)(2,1)S(1)}, bf16[128,256]{1,0:T(8,128)(2,1)S(1)}, u32[]{:S(2)}, u32[]{:S(2)}) collective-permute-start(bf16[128,256]{1,0:T(8,128)(2,1)S(1)} %get-tuple-element.29), channel_id=1, source_target_pairs={{0,1},{1,2},{2,3},{3,0},{4,5},{5,6},{6,7},{7,4},{8,9},{9,10},{10,1... | collective-permute-start | bytes 196616 | tf_op jit(solution)/shard_map/ppermute | solution.py:315
  3.7 7.3 %collective-permute-start.5 = (bf16[128,256]{1,0:T(8,128)(2,1)S(1)}, bf16[128,256]{1,0:T(8,128)(2,1)S(1)}, u32[]{:S(2)}, u32[]{:S(2)}) collective-permute-start(bf16[128,256]{1,0:T(8,128)(2,1)S(1)} %get-tuple-element.30), channel_id=1, source_target_pairs={{0,2},{1,3},{2,0},{3,1},{4,6},{5,7},{6,4},{7,5},{8,10},{9,11},{10,... | collective-permute-start | bytes 196616 | tf_op jit(solution)/shard_map/ppermute | solution.py:315
  6.5 4.6 %collective-permute-start.6 = (bf16[128,256]{1,0:T(8,128)(2,1)S(1)}, bf16[128,256]{1,0:T(8,128)(2,1)S(1)}, u32[]{:S(2)}, u32[]{:S(2)}) collective-permute-start(bf16[128,256]{1,0:T(8,128)(2,1)S(1)} %get-tuple-element.31), channel_id=1, source_target_pairs={{0,3},{1,0},{2,1},{3,2},{4,7},{5,4},{6,5},{7,6},{8,11},{9,8},{10,9... | collective-permute-start | bytes 196616 | tf_op jit(solution)/shard_map/ppermute | solution.py:315
  8.7 2.3 copy-start.2
  8.7 2.3 copy-start.3
  8.7 2.3 copy-start.4
  14.8 63.5 %all-to-all-start.2 = ((bf16[64,8,2048]{2,1,0:T(8,128)(2,1)}), bf16[64,8,2048]{2,1,0:T(8,128)(2,1)}, u32[]{:S(2)}, u32[]{:S(2)}) async-start(bf16[64,8,2048]{2,1,0:T(8,128)(2,1)} %bitcast.60), calls=%async_computation.2 | async-start | bytes 4194304 | tf_op jit(solution)/shard_map/all_to_all | solution.py:286
  27.1 6.0 %collective-permute-start = (bf16[32,256]{1,0:T(8,128)(2,1)S(1)}, bf16[32,256]{1,0:T(8,128)(2,1)S(1)}, u32[]{:S(2)}, u32[]{:S(2)}) collective-permute-start(bf16[32,256]{1,0:T(8,128)(2,1)S(1)} %get-tuple-element.20), channel_id=1, source_target_pairs={{0,4},{4,8},{8,12},{12,16},{16,20},{20,24},{24,28},{28,32},{32,36}... | collective-permute-start | bytes 49160 | tf_op jit(solution)/shard_map/ppermute | solution.py:319
  35.1 5.7 %collective-permute-start.1 = (bf16[128,256]{1,0:T(8,128)(2,1)S(1)}, bf16[128,256]{1,0:T(8,128)(2,1)S(1)}, u32[]{:S(2)}, u32[]{:S(2)}) collective-permute-start(bf16[128,256]{1,0:T(8,128)(2,1)S(1)} %get-tuple-element.22), channel_id=1, source_target_pairs={{0,1},{1,2},{2,3},{3,0},{4,5},{5,6},{6,7},{7,4},{8,9},{9,10},{10,1... | collective-permute-start | bytes 196616 | tf_op jit(solution)/shard_map/ppermute | solution.py:315
  35.8 6.1 %collective-permute-start.2 = (bf16[128,256]{1,0:T(8,128)(2,1)S(1)}, bf16[128,256]{1,0:T(8,128)(2,1)S(1)}, u32[]{:S(2)}, u32[]{:S(2)}) collective-permute-start(bf16[128,256]{1,0:T(8,128)(2,1)S(1)} %get-tuple-element.23), channel_id=1, source_target_pairs={{0,2},{1,3},{2,0},{3,1},{4,6},{5,7},{6,4},{7,5},{8,10},{9,11},{10,... | collective-permute-start | bytes 196616 | tf_op jit(solution)/shard_map/ppermute | solution.py:315
  39.0 4.3 %collective-permute-start.3 = (bf16[128,256]{1,0:T(8,128)(2,1)S(1)}, bf16[128,256]{1,0:T(8,128)(2,1)S(1)}, u32[]{:S(2)}, u32[]{:S(2)}) collective-permute-start(bf16[128,256]{1,0:T(8,128)(2,1)S(1)} %get-tuple-element.24), channel_id=1, source_target_pairs={{0,3},{1,0},{2,1},{3,2},{4,7},{5,4},{6,5},{7,6},{8,11},{9,8},{10,9... | collective-permute-start | bytes 196616 | tf_op jit(solution)/shard_map/ppermute | solution.py:315
  48.7 1.3 copy-start.1
  78.3 72.1 %all-to-all-start = ((bf16[64,8,2048]{2,1,0:T(8,128)(2,1)}), bf16[64,8,2048]{2,1,0:T(8,128)(2,1)}, u32[]{:S(2)}, u32[]{:S(2)}) async-start(bf16[64,8,2048]{2,1,0:T(8,128)(2,1)} %bitcast.55), calls=%async_computation | async-start | bytes 4194304 | tf_op jit(solution)/shard_map/all_to_all | solution.py:286
  150.3 56.8 %all-to-all-start.3 = ((bf16[64,8,2048]{2,1,0:T(8,128)(2,1)}), bf16[64,8,2048]{2,1,0:T(8,128)(2,1)}, u32[]{:S(2)}, u32[]{:S(2)}) async-start(bf16[64,8,2048]{2,1,0:T(8,128)(2,1)} %fusion.1), calls=%async_computation.3 | async-start | bytes 4194304 | tf_op jit(solution)/shard_map/all_to_all | solution.py:286
  165.4 47.3 %copy-start.6 = (bf16[2048,4]{0,1:T(4,128)(2,1)S(1)}, bf16[2048,4]{0,1:T(4,128)(2,1)}, u32[]{:S(2)}) copy-start(bf16[2048,4]{0,1:T(4,128)(2,1)} %param.24) | copy-start | bytes 49156
  165.4 48.4 %copy-start.5 = (bf16[2048,64]{0,1:T(8,128)(2,1)S(1)}, bf16[2048,64]{0,1:T(8,128)(2,1)}, u32[]{:S(2)}) copy-start(bf16[2048,64]{0,1:T(8,128)(2,1)} %param.25) | copy-start | bytes 786436
  207.1 56.8 %all-to-all-start.1 = ((bf16[64,8,2048]{2,1,0:T(8,128)(2,1)}), bf16[64,8,2048]{2,1,0:T(8,128)(2,1)}, u32[]{:S(2)}, u32[]{:S(2)}) async-start(bf16[64,8,2048]{2,1,0:T(8,128)(2,1)} %fusion), calls=%async_computation.1 | async-start | bytes 4194304 | tf_op jit(solution)/shard_map/all_to_all | solution.py:286
where the time goes:
time: 268 us
  waiting for transfers between devices  157 us (59%)
  starting transfers between devices  56.2 us (21%)
  Pallas kernels  31.2 us (12%)
  matrix products  19 us (7%)
  local copies, waits for them, and re-layouts  4.22 us (2%)
    all_to_all x4, waiting for transfers between devices, exchange(): lax.all_to_all(blocks, 'sp', split_axis=0, concat_axis=0, tiled=True)  149 us
    all_to_all x4, starting transfers between devices, exchange(): lax.all_to_all(blocks, 'sp', split_axis=0, concat_axis=0, tiled=True)  44.5 us
    dot_general x2, matrix products, expert_ffn(): jnp.dot(hidden, expert_down[0], preferred_element_type=f32).astype(bf16)  12.1 us
    ppermute x6, starting transfers between devices, on_device(): lax.ppermute(blocks[d], 'tp', [(i, (i + d) % 4) for i in range(4)])  9.66 us
    pallas_call x2, Pallas kernels, mix(): pl.pallas_call(functools.partial(mix_kernel, half), out_shape=jax.ShapeDt...  9.19 us
    pallas_call x2, Pallas kernels, weights(): pl.pallas_call(functools.partial(weight_kernel, half), out_shape=[jax.Sha...  8.4 us
    pallas_call x2, Pallas kernels, finish(): pl.pallas_call(finish_kernel, grid=(1,), out_shape=jax.ShapeDtypeStruct((...  7.22 us
    dot_general x2, matrix products, expert_ffn(): up_out = jnp.dot(arrived, expert_up[0], preferred_element_type=f32)  6.93 us
  transfers between devices with their start and end apart: 11, of which 8 were waited for; matrix products, arithmetic and copies ran while one was open for 8% of the time, Pallas kernels for 8%

commit v1 on v0

--- a/solution.py
+++ b/solution.py
@@ -39,6 +39,8 @@
 def pool_kernel(half, *refs):
     if half == 0:
         tail, refs = refs[0], refs[1:]
+    else:
+        weight, refs = refs[0], refs[1:]
     x, docs_in, map_in, scale_in, out0, out1, out2, out3 = refs[:8]
     xs, ds, docs, pool_map, scale, sems = refs[-6:]
     tp, sp = lax.axis_index("tp"), lax.axis_index("sp")
@@ -50,6 +52,9 @@
     ]
     for load in loads:
         load.start()
+    if half == 1:
+        fetch = pltpu.make_async_copy(weight, refs[9], sems.at[4])
+        fetch.start()
     if half == 0:
         xs[0 : BLK - TAIL, :] = jnp.zeros((BLK - TAIL, CHANNELS), bf16)
         xs[BLK - TAIL : BLK, :] = tail[0:TAIL, :]
@@ -89,18 +94,20 @@
         message[0:TAIL, :] = xs[BLK + x.shape[0] - TAIL :, :]
         message[TAIL:, 0:BLK] = jnp.broadcast_to(ds[8:9, :], (TAIL, BLK)).astype(bf16)
         message[TAIL:, BLK:] = jnp.zeros((TAIL, CHANNELS - BLK), bf16)
-
-
-def pool(half, x, docs, pool_map, scale, tail=None):
+        fetch.wait()
+
+
+def pool(half, x, docs, pool_map, scale, tail=None, weight=None):
     rows = x.shape[0]
     shapes = [jax.ShapeDtypeStruct((HALF, CHANNELS), bf16)] * 4
     if half == 1:
         shapes.append(jax.ShapeDtypeStruct((2 * TAIL, CHANNELS), bf16))
-    first = [] if tail is None else [tail]
+        shapes.append(jax.ShapeDtypeStruct(weight.shape, bf16))
+    first = tail if half == 0 else in_hbm(weight)
     return pl.pallas_call(
         functools.partial(pool_kernel, half),
         out_shape=shapes,
-        in_specs=[VMEM] * len(first) + [HBM] * 4,
+        in_specs=[VMEM if half == 0 else HBM] + [HBM] * 4,
         out_specs=[VMEM] * len(shapes),
         scratch_shapes=[
             pltpu.VMEM((rows + BLK, CHANNELS), bf16),
@@ -108,14 +115,18 @@
             pltpu.VMEM(docs.shape, jnp.int32),
             pltpu.VMEM(pool_map.shape, bf16),
             pltpu.VMEM(scale.shape, f32),
-            pltpu.SemaphoreType.DMA((4,)),
+            pltpu.SemaphoreType.DMA((5,)),
         ],
         name="pool",
         compiler_params=ROOM,
-    )(*first, *in_hbm(x, docs, pool_map, scale))
-
-
-def slots_of(chosen):
+    )(first, *in_hbm(x, docs, pool_map, scale))
+
+
+def slots_of(routes, half):
+    def column(k):
+        row = routes[k : k + 1, half * HALF : (half + 1) * HALF].astype(f32)
+        return jnp.transpose(jnp.broadcast_to(row, (HALF, HALF)))[:, 0:1].astype(jnp.int32)
+
     strict = (
         lax.broadcasted_iota(jnp.int32, (HALF, HALF), 1)
         < lax.broadcasted_iota(jnp.int32, (HALF, HALF), 0)
@@ -123,7 +134,7 @@
     strict = jnp.where(strict, 1.0, 0.0).astype(bf16)
     expert = lax.broadcasted_iota(jnp.int32, (HALF, EXPERTS), 1)
     slot = lax.broadcasted_iota(jnp.int32, (HALF, SLOTS), 1)
-    first, second = chosen[:, 0:1], chosen[:, 1:2]
+    first, second = column(0), column(1)
     hot0 = jnp.where(expert == first, 1.0, 0.0)
     hot1 = jnp.where(expert == second, 1.0, 0.0)
     before0 = dot(strict, hot0.astype(bf16))
@@ -133,29 +144,20 @@
     return slot == first * 8 + rank0, slot == second * 8 + rank1
 
 
-def slot_kernel(routes, weight, gather, near_weight, sem):
-    load = pltpu.make_async_copy(weight, near_weight, sem)
-    load.start()
-    for h in range(2):
-        hit0, hit1 = slots_of(routes[h * HALF : (h + 1) * HALF, :])
-        hit = jnp.where(hit0 | hit1, 1.0, 0.0)
-        gather[h] = jnp.transpose(hit).astype(bf16)
-    load.wait()
-
-
-def slots(routes, weight):
-    return pl.pallas_call(
-        slot_kernel,
-        out_shape=[
-            jax.ShapeDtypeStruct((2, SLOTS, HALF), bf16),
-            jax.ShapeDtypeStruct(weight.shape, bf16),
-        ],
-        in_specs=[VMEM, HBM],
-        out_specs=[VMEM] * 2,
-        scratch_shapes=[pltpu.SemaphoreType.DMA],
+def slot_kernel(half, routes, gather):
+    hit0, hit1 = slots_of(routes, half)
+    gather[...] = jnp.transpose(jnp.where(hit0 | hit1, 1.0, 0.0)).astype(bf16)
+
+
+def slots(half, routes):
+    return pl.pallas_call(
+        functools.partial(slot_kernel, half),
+        out_shape=jax.ShapeDtypeStruct((SLOTS, HALF), bf16),
+        in_specs=[VMEM],
+        out_specs=VMEM,
         name="slots",
         compiler_params=ROOM,
-    )(routes, weight)
+    )(routes)
 
 
 def norm(values, gain, shift):
@@ -183,7 +185,7 @@
     stores = []
     for c in range(CHUNKS):
         part = slice(c * SLOTS // CHUNKS, (c + 1) * SLOTS // CHUNKS)
-        rows[part, :] = dot(gather[half, part, :], normed).astype(bf16)
+        rows[part, :] = dot(gather[part, :], normed).astype(bf16)
         stores.append(pltpu.make_async_copy(rows.at[part, :], rows_out.at[part, :], sems.at[c]))
         stores[-1].start()
     for store in stores:
@@ -207,7 +209,7 @@
 
 
 def weight_kernel(half, laid_out, group_router, expert_router, routes, normed, split):
-    hit0, hit1 = slots_of(routes[half * HALF : (half + 1) * HALF, :])
+    hit0, hit1 = slots_of(routes, half)
     rows = dot(jnp.where(hit0, 1.0, 0.0).astype(bf16), laid_out[...]).astype(bf16)
     normed[...] = rows
     group_logits = dot(rows, group_router[...])
@@ -308,19 +310,20 @@
     sp_count = lax.axis_size("sp")
     docs = doc_ids.reshape(doc_ids.shape[0] // BLK, BLK)
     inputs = (pool_input, docs, pool_map, pool_scale[None, :])
+    flat_routes = routes.T
     parts, tail = {}, None
     for h in (1, 0):
-        blocks = pool(h, *inputs, tail=tail)
+        blocks = pool(h, *inputs, tail=tail, weight=out_weight)
         parts[h] = [blocks[0]] + [
             lax.ppermute(blocks[d], "tp", [(i, (i + d) % 4) for i in range(4)])
             for d in range(1, 4)
         ]
         if h == 1:
             tail = lax.ppermute(blocks[4], "sp", [(i, i + 1) for i in range(sp_count - 1)])
-            gather, near_weight = slots(routes, out_weight)
-            near_weight = pltpu.with_memory_space_constraint(near_weight, pltpu.VMEM)
+            near_weight = pltpu.with_memory_space_constraint(blocks[5], pltpu.VMEM)
     arrived, kept = {}, {}
     for h in (1, 0):
+        gather = slots(h, flat_routes)
         outgoing = mix(
             h,
             parts[h],
@@ -331,7 +334,7 @@
             gather,
         )
         arrived[h] = exchange(outgoing)
-        kept[h] = weights(h, outgoing, group_router, expert_router, routes)
+        kept[h] = weights(h, outgoing, group_router, expert_router, flat_routes)
     result = None
     for h in (1, 0):
         returned = exchange(expert_ffn(arrived[h], expert_gate, expert_up, expert_down))

time: 268 us -> 269 us (level)
  transfers between devices with their start and end apart: 11 -> 11, of which waited for: 8 -> 10; matrix products, arithmetic and copies ran while one was open for 8% -> 8% of each run, Pallas kernels for 8% -> 8%
where the time goes in v1:
time: 269 us; the launch traced here: 268 us
  waiting for transfers between devices  158 us (59%)
  starting transfers between devices  56.9 us (21%)
  Pallas kernels  30.6 us (11%)
  matrix products  19 us (7%)
  local copies, waits for them, and re-layouts  3.41 us (1%)
    all_to_all x4, waiting for transfers between devices, exchange(): lax.all_to_all(blocks, 'sp', split_axis=0, concat_axis=0, tiled=True)  148 us
    all_to_all x4, starting transfers between devices, exchange(): lax.all_to_all(blocks, 'sp', split_axis=0, concat_axis=0, tiled=True)  44.9 us
    dot_general x2, matrix products, expert_ffn(): jnp.dot(hidden, expert_down[0], preferred_element_type=f32).astype(bf16)  12.1 us
    ppermute x6, starting transfers between devices, on_device(): lax.ppermute(blocks[d], 'tp', [(i, (i + d) % 4) for i in range(4)])  10 us
    pallas_call x2, Pallas kernels, mix(): pl.pallas_call(functools.partial(mix_kernel, half), out_shape=jax.ShapeDt...  9.13 us
    pallas_call x2, Pallas kernels, weights(): pl.pallas_call(functools.partial(weight_kernel, half), out_shape=[jax.Sha...  8.51 us
    pallas_call x2, Pallas kernels, finish(): pl.pallas_call(finish_kernel, grid=(1,), out_shape=jax.ShapeDtypeStruct((...  7.22 us
    dot_general x2, matrix products, expert_ffn(): up_out = jnp.dot(arrived, expert_up[0], preferred_element_type=f32)  6.93 us
  transfers between devices with their start and end apart: 11, of which 10 were waited for; matrix products, arithmetic and copies ran while one was open for 8% of the time, Pallas kernels for 8%

profile of v1, /device:TPU:8, one launch (start us, length us, event | category | flops | bytes accessed | tf_op | source)
XLA Modules:
  0.0 268.0 jit_solution(16553066236647874470)
XLA Ops:
  0.0 0.0 copy-start
  0.0 0.0 copy-start.2
  0.0 0.0 copy-start.3
  0.0 0.0 copy-start.4
  0.0 2.6 pool.2
  2.6 1.6 collective-permute-start.4
  4.2 2.7 %collective-permute-start.5 = (bf16[128,256]{1,0:T(8,128)(2,1)S(1)}, bf16[128,256]{1,0:T(8,128)(2,1)S(1)}, u32[]{:S(2)}, u32[]{:S(2)}) collective-permute-start(bf16[128,256]{1,0:T(8,128)(2,1)S(1)} %get-tuple-element.28), channel_id=1, source_target_pairs={{0,2},{1,3},{2,0},{3,1},{4,6},{5,7},{6,4},{7,5},{8,10},{9,11},{10,... | collective-permute-start | bytes 196616 | tf_op jit(solution)/shard_map/ppermute | solution.py:318
  6.9 1.4 collective-permute-start.6
  8.4 0.0 copy-done.2
  8.4 0.5 slots.3.gather
  8.9 0.0 collective-permute-done.4.m1
  8.9 1.2 collective-permute-done.5.m2
  10.1 1.1 collective-permute-done.6.m3
  11.2 0.0 copy-done.3
  11.2 0.0 copy-done.4
  11.2 3.6 %mix.3.laid_out = bf16[512,2048]{1,0:T(8,128)(2,1)} custom-call(bf16[128,256]{1,0:T(8,128)(2,1)S(1)} %get-tuple-element.26.m0, bf16[128,256]{1,0:T(8,128)(2,1)S(1)} %collective-permute-done.4.m1, bf16[128,256]{1,0:T(8,128)(2,1)S(1)} %collective-permute-done.5.m2, bf16[128,256]{1,0:T(8,128)(2,1)S(1)} %collective-permute-done.6.m3, ...), custom_call_target="tpu_custom_call" | custom-call | tf_op jit(solution)/shard_map/mix/pallas_call | solution.py:196
  14.9 12.3 %all-to-all-start.2 = ((bf16[64,8,2048]{2,1,0:T(8,128)(2,1)}), bf16[64,8,2048]{2,1,0:T(8,128)(2,1)}, u32[]{:S(2)}, u32[]{:S(2)}) async-start(bf16[64,8,2048]{2,1,0:T(8,128)(2,1)} %bitcast.65), calls=%async_computation.2 | async-start | bytes 4194304 | tf_op jit(solution)/shard_map/all_to_all | solution.py:288
  27.2 2.0 collective-permute-start
  29.2 4.0 %collective-permute-done.refs_0_ = bf16[32,256]{1,0:T(8,128)(2,1)S(1)} collective-permute-done((bf16[32,256]{1,0:T(8,128)(2,1)S(1)}, bf16[32,256]{1,0:T(8,128)(2,1)S(1)}, u32[]{:S(2)}, u32[]{:S(2)}) %collective-permute-start) | collective-permute-done | bytes 16416 | tf_op jit(solution)/shard_map/ppermute | solution.py:322
  33.2 2.0 pool.3
  35.2 0.7 collective-permute-start.1
  35.9 3.5 %collective-permute-start.2 = (bf16[128,256]{1,0:T(8,128)(2,1)S(1)}, bf16[128,256]{1,0:T(8,128)(2,1)S(1)}, u32[]{:S(2)}, u32[]{:S(2)}) collective-permute-start(bf16[128,256]{1,0:T(8,128)(2,1)S(1)} %get-tuple-element.22), channel_id=1, source_target_pairs={{0,2},{1,3},{2,0},{3,1},{4,6},{5,7},{6,4},{7,5},{8,10},{9,11},{10,... | collective-permute-start | bytes 196616 | tf_op jit(solution)/shard_map/ppermute | solution.py:318
  39.4 0.1 collective-permute-start.3
  39.5 0.6 slots.2.gather
  40.1 1.3 collective-permute-done.1.m1
  41.3 1.0 collective-permute-done.2.m2
  42.3 1.3 collective-permute-done.3.m3
  43.7 5.5 %mix.2.laid_out = bf16[512,2048]{1,0:T(8,128)(2,1)S(1)} custom-call(bf16[128,256]{1,0:T(8,128)(2,1)S(1)} %get-tuple-element.20.m0, bf16[128,256]{1,0:T(8,128)(2,1)S(1)} %collective-permute-done.1.m1, bf16[128,256]{1,0:T(8,128)(2,1)S(1)} %collective-permute-done.2.m2, bf16[128,256]{1,0:T(8,128)(2,1)S(1)} %collective-permute-done.3.m3, ...), custom_call_target="tpu_custom_call" | custom-call | tf_op jit(solution)/shard_map/mix/pallas_call | solution.py:196
  49.2 0.0 copy-start.1
  49.2 1.3 copy-done.1
  50.5 27.8 %all-to-all-done.2 = bf16[64,8,2048]{2,1,0:T(8,128)(2,1)} async-done(((bf16[64,8,2048]{2,1,0:T(8,128)(2,1)}), bf16[64,8,2048]{2,1,0:T(8,128)(2,1)}, u32[]{:S(2)}, u32[]{:S(2)}) %all-to-all-start.2) | async-done | bytes 2097184 | tf_op jit(solution)/shard_map/all_to_all | solution.py:288
  78.3 21.3 %all-to-all-start = ((bf16[64,8,2048]{2,1,0:T(8,128)(2,1)}), bf16[64,8,2048]{2,1,0:T(8,128)(2,1)}, u32[]{:S(2)}, u32[]{:S(2)}) async-start(bf16[64,8,2048]{2,1,0:T(8,128)(2,1)} %bitcast.56), calls=%async_computation | async-start | bytes 4194304 | tf_op jit(solution)/shard_map/all_to_all | solution.py:288
  99.6 3.5 %fusion.2 = f32[512,512]{1,0:T(8,128)S(1)} fusion(bf16[64,8,2048]{2,1,0:T(8,128)(2,1)} %all-to-all-done.2, bf16[1,2048,512]{2,1,0:T(8,128)(2,1)} %param.27), kind=kOutput, calls=%fused_computation.4 | convolution fusion | flops 1073741824 | bytes 5242880 | tf_op jit(solution)/shard_map/dot_general | solution.py:281
  103.1 0.0 copy-done
  103.1 6.1 %fusion.1 = bf16[64,8,2048]{2,1,0:T(8,128)(2,1)} fusion(bf16[1,512,2048]{2,1,0:T(8,128)(2,1)S(1)} %copy-done, f32[512,512]{1,0:T(8,128)S(1)} %fusion.2, bf16[64,8,2048]{2,1,0:T(8,128)(2,1)} %all-to-all-done.2, bf16[1,2048,512]{2,1,0:T(8,128)(2,1)} %param.26), kind=kOutput, calls=%fused_computation.3 | convolution fusion | flops 2150105088 | bytes 9437184 | tf_op jit(solution)/shard_map/dot_general | solution.py:283
  109.2 41.6 %all-to-all-done = bf16[64,8,2048]{2,1,0:T(8,128)(2,1)} async-done(((bf16[64,8,2048]{2,1,0:T(8,128)(2,1)}), bf16[64,8,2048]{2,1,0:T(8,128)(2,1)}, u32[]{:S(2)}, u32[]{:S(2)}) %all-to-all-start) | async-done | bytes 2097184 | tf_op jit(solution)/shard_map/all_to_all | solution.py:288
  150.8 5.6 %all-to-all-start.3 = ((bf16[64,8,2048]{2,1,0:T(8,128)(2,1)}), bf16[64,8,2048]{2,1,0:T(8,128)(2,1)}, u32[]{:S(2)}, u32[]{:S(2)}) async-start(bf16[64,8,2048]{2,1,0:T(8,128)(2,1)} %fusion.1), calls=%async_computation.3 | async-start | bytes 4194304 | tf_op jit(solution)/shard_map/all_to_all | solution.py:288
  156.4 3.5 %fusion.9 = f32[512,512]{1,0:T(8,128)S(1)} fusion(bf16[1,2048,512]{2,1,0:T(8,128)(2,1)} %param.27, bf16[64,8,2048]{2,1,0:T(8,128)(2,1)} %all-to-all-done), kind=kOutput, calls=%fused_computation.11 | convolution fusion | flops 1073741824 | bytes 5242880 | tf_op jit(solution)/shard_map/dot_general | solution.py:281
  159.9 6.0 %fusion = bf16[64,8,2048]{2,1,0:T(8,128)(2,1)} fusion(bf16[1,512,2048]{2,1,0:T(8,128)(2,1)S(1)} %copy-done, f32[512,512]{1,0:T(8,128)S(1)} %fusion.9, bf16[1,2048,512]{2,1,0:T(8,128)(2,1)} %param.26, bf16[64,8,2048]{2,1,0:T(8,128)(2,1)} %all-to-all-done), kind=kOutput, calls=%fused_computation.2 | convolution fusion | flops 2150105088 | bytes 9437184 | tf_op jit(solution)/shard_map/dot_general | solution.py:283
  165.9 0.0 copy-start.6
  165.9 0.0 copy-start.5
  165.9 41.6 %all-to-all-done.3 = bf16[64,8,2048]{2,1,0:T(8,128)(2,1)} async-done(((bf16[64,8,2048]{2,1,0:T(8,128)(2,1)}), bf16[64,8,2048]{2,1,0:T(8,128)(2,1)}, u32[]{:S(2)}, u32[]{:S(2)}) %all-to-all-start.3) | async-done | bytes 2097184 | tf_op jit(solution)/shard_map/all_to_all | solution.py:288
  207.6 5.6 %all-to-all-start.1 = ((bf16[64,8,2048]{2,1,0:T(8,128)(2,1)}), bf16[64,8,2048]{2,1,0:T(8,128)(2,1)}, u32[]{:S(2)}, u32[]{:S(2)}) async-start(bf16[64,8,2048]{2,1,0:T(8,128)(2,1)} %fusion), calls=%async_computation.1 | async-start | bytes 4194304 | tf_op jit(solution)/shard_map/all_to_all | solution.py:288
  213.2 0.0 copy-done.6
  213.2 1.1 copy.18.group_router
  214.3 0.0 copy-done.5
  214.3 1.0 copy.19.expert_router
  215.3 4.3 %weights.3 = (bf16[128,2048]{1,0:T(8,128)(2,1)}, bf16[256,512]{1,0:T(8,128)(2,1)}) custom-call(bf16[512,2048]{1,0:T(8,128)(2,1)} %mix.3.laid_out, bf16[2048,4]{1,0:T(8,128)(2,1)} %copy.18.group_router, bf16[2048,64]{1,0:T(8,128)(2,1)} %copy.19.expert_router, s32[2,256]{1,0:T(2,128)} %bitcast.57), custom_call_target="tpu_custom_call" | custom-call | tf_op jit(solution)/shard_map/weights/pallas_call | solution.py:237
  219.5 4.3 %weights.2 = (bf16[128,2048]{1,0:T(8,128)(2,1)}, bf16[256,512]{1,0:T(8,128)(2,1)}) custom-call(bf16[512,2048]{1,0:T(8,128)(2,1)} %copy-done.1, bf16[2048,4]{1,0:T(8,128)(2,1)} %copy.18.group_router, bf16[2048,64]{1,0:T(8,128)(2,1)} %copy.19.expert_router, s32[2,256]{1,0:T(2,128)} %bitcast.58), custom_call_target="tpu_custom_call" | custom-call | tf_op jit(solution)/shard_map/weights/pallas_call | solution.py:237
  223.8 3.6 %finish.2.rest_0_ = bf16[256,2048]{1,0:T(8,128)(2,1)} custom-call(bf16[256,512]{1,0:T(8,128)(2,1)} %get-tuple-element.31.split, bf16[512,2048]{1,0:T(8,128)(2,1)} %bitcast.17.returned, bf16[128,2048]{1,0:T(8,128)(2,1)} %get-tuple-element.32.normed, f32[1,2048]{1,0:T(1,128)} %bitcast.66, f32[1,2048]{1,0:T(1,128)} %bitcast.68), custom_call_target="tpu_custom_call" | custom-call | tf_op jit(solution)/shard_map/finish/pallas_call | solution.py:268
  227.4 37.0 %all-to-all-done.1 = bf16[64,8,2048]{2,1,0:T(8,128)(2,1)} async-done(((bf16[64,8,2048]{2,1,0:T(8,128)(2,1)}), bf16[64,8,2048]{2,1,0:T(8,128)(2,1)}, u32[]{:S(2)}, u32[]{:S(2)}) %all-to-all-start.1) | async-done | bytes 2097184 | tf_op jit(solution)/shard_map/all_to_all | solution.py:288
  264.4 3.6 %finish.3 = bf16[256,2048]{1,0:T(8,128)(2,1)} custom-call(bf16[256,512]{1,0:T(8,128)(2,1)} %get-tuple-element.24.split, bf16[512,2048]{1,0:T(8,128)(2,1)} %bitcast.11.returned, bf16[128,2048]{1,0:T(8,128)(2,1)} %get-tuple-element.25.normed, f32[1,2048]{1,0:T(1,128)} %bitcast.67, f32[1,2048]{1,0:T(1,128)} %bitcast.69, ...), custom_call_target="tpu_custom_call", output_to_operand_aliasing={{}: (5, {})} | custom-call | tf_op jit(solution)/shard_map/finish/pallas_call | solution.py:268
Async XLA Ops:
  0.0 103.1 %copy-start = (bf16[1,512,2048]{2,1,0:T(8,128)(2,1)S(1)}, bf16[1,512,2048]{2,1,0:T(8,128)(2,1)}, u32[]{:S(2)}) copy-start(bf16[1,512,2048]{2,1,0:T(8,128)(2,1)} %param.28) | copy-start | bytes 6291460
  0.0 8.4 %copy-start.2 = (s32[256,2]{0,1:T(2,128)S(1)}, s32[256,2]{0,1:T(2,128)}, u32[]{:S(2)}) copy-start(s32[256,2]{0,1:T(2,128)} %param.29) | copy-start | bytes 6148
  0.0 11.2 %copy-start.3 = (f32[2048]{0:T(1024)S(1)}, f32[2048]{0:T(1024)}, u32[]{:S(2)}) copy-start(f32[2048]{0:T(1024)} %param.22) | copy-start | bytes 24580
  0.0 11.2 %copy-start.4 = (f32[2048]{0:T(1024)S(1)}, f32[2048]{0:T(1024)}, u32[]{:S(2)}) copy-start(f32[2048]{0:T(1024)} %param.23) | copy-start | bytes 24580
  2.6 6.3 %collective-permute-start.4 = (bf16[128,256]{1,0:T(8,128)(2,1)S(1)}, bf16[128,256]{1,0:T(8,128)(2,1)S(1)}, u32[]{:S(2)}, u32[]{:S(2)}) collective-permute-start(bf16[128,256]{1,0:T(8,128)(2,1)S(1)} %get-tuple-element.27), channel_id=1, source_target_pairs={{0,1},{1,2},{2,3},{3,0},{4,5},{5,6},{6,7},{7,4},{8,9},{9,10},{10,1... | collective-permute-start | bytes 196616 | tf_op jit(solution)/shard_map/ppermute | solution.py:318
  4.2 5.9 %collective-permute-start.5 = (bf16[128,256]{1,0:T(8,128)(2,1)S(1)}, bf16[128,256]{1,0:T(8,128)(2,1)S(1)}, u32[]{:S(2)}, u32[]{:S(2)}) collective-permute-start(bf16[128,256]{1,0:T(8,128)(2,1)S(1)} %get-tuple-element.28), channel_id=1, source_target_pairs={{0,2},{1,3},{2,0},{3,1},{4,6},{5,7},{6,4},{7,5},{8,10},{9,11},{10,... | collective-permute-start | bytes 196616 | tf_op jit(solution)/shard_map/ppermute | solution.py:318
  6.9 4.3 %collective-permute-start.6 = (bf16[128,256]{1,0:T(8,128)(2,1)S(1)}, bf16[128,256]{1,0:T(8,128)(2,1)S(1)}, u32[]{:S(2)}, u32[]{:S(2)}) collective-permute-start(bf16[128,256]{1,0:T(8,128)(2,1)S(1)} %get-tuple-element.29), channel_id=1, source_target_pairs={{0,3},{1,0},{2,1},{3,2},{4,7},{5,4},{6,5},{7,6},{8,11},{9,8},{10,9... | collective-permute-start | bytes 196616 | tf_op jit(solution)/shard_map/ppermute | solution.py:318
  14.9 63.5 %all-to-all-start.2 = ((bf16[64,8,2048]{2,1,0:T(8,128)(2,1)}), bf16[64,8,2048]{2,1,0:T(8,128)(2,1)}, u32[]{:S(2)}, u32[]{:S(2)}) async-start(bf16[64,8,2048]{2,1,0:T(8,128)(2,1)} %bitcast.65), calls=%async_computation.2 | async-start | bytes 4194304 | tf_op jit(solution)/shard_map/all_to_all | solution.py:288
  27.2 6.0 %collective-permute-start = (bf16[32,256]{1,0:T(8,128)(2,1)S(1)}, bf16[32,256]{1,0:T(8,128)(2,1)S(1)}, u32[]{:S(2)}, u32[]{:S(2)}) collective-permute-start(bf16[32,256]{1,0:T(8,128)(2,1)S(1)} %get-tuple-element.19), channel_id=1, source_target_pairs={{0,4},{4,8},{8,12},{12,16},{16,20},{20,24},{24,28},{28,32},{32,36}... | collective-permute-start | bytes 49160 | tf_op jit(solution)/shard_map/ppermute | solution.py:322
  35.2 6.1 %collective-permute-start.1 = (bf16[128,256]{1,0:T(8,128)(2,1)S(1)}, bf16[128,256]{1,0:T(8,128)(2,1)S(1)}, u32[]{:S(2)}, u32[]{:S(2)}) collective-permute-start(bf16[128,256]{1,0:T(8,128)(2,1)S(1)} %get-tuple-element.21), channel_id=1, source_target_pairs={{0,1},{1,2},{2,3},{3,0},{4,5},{5,6},{6,7},{7,4},{8,9},{9,10},{10,1... | collective-permute-start | bytes 196616 | tf_op jit(solution)/shard_map/ppermute | solution.py:318
  35.9 6.5 %collective-permute-start.2 = (bf16[128,256]{1,0:T(8,128)(2,1)S(1)}, bf16[128,256]{1,0:T(8,128)(2,1)S(1)}, u32[]{:S(2)}, u32[]{:S(2)}) collective-permute-start(bf16[128,256]{1,0:T(8,128)(2,1)S(1)} %get-tuple-element.22), channel_id=1, source_target_pairs={{0,2},{1,3},{2,0},{3,1},{4,6},{5,7},{6,4},{7,5},{8,10},{9,11},{10,... | collective-permute-start | bytes 196616 | tf_op jit(solution)/shard_map/ppermute | solution.py:318
  39.4 4.3 %collective-permute-start.3 = (bf16[128,256]{1,0:T(8,128)(2,1)S(1)}, bf16[128,256]{1,0:T(8,128)(2,1)S(1)}, u32[]{:S(2)}, u32[]{:S(2)}) collective-permute-start(bf16[128,256]{1,0:T(8,128)(2,1)S(1)} %get-tuple-element.23), channel_id=1, source_target_pairs={{0,3},{1,0},{2,1},{3,2},{4,7},{5,4},{6,5},{7,6},{8,11},{9,8},{10,9... | collective-permute-start | bytes 196616 | tf_op jit(solution)/shard_map/ppermute | solution.py:318
  49.2 1.3 copy-start.1
  78.3 72.5 %all-to-all-start = ((bf16[64,8,2048]{2,1,0:T(8,128)(2,1)}), bf16[64,8,2048]{2,1,0:T(8,128)(2,1)}, u32[]{:S(2)}, u32[]{:S(2)}) async-start(bf16[64,8,2048]{2,1,0:T(8,128)(2,1)} %bitcast.56), calls=%async_computation | async-start | bytes 4194304 | tf_op jit(solution)/shard_map/all_to_all | solution.py:288
  150.8 56.8 %all-to-all-start.3 = ((bf16[64,8,2048]{2,1,0:T(8,128)(2,1)}), bf16[64,8,2048]{2,1,0:T(8,128)(2,1)}, u32[]{:S(2)}, u32[]{:S(2)}) async-start(bf16[64,8,2048]{2,1,0:T(8,128)(2,1)} %fusion.1), calls=%async_computation.3 | async-start | bytes 4194304 | tf_op jit(solution)/shard_map/all_to_all | solution.py:288
  165.9 47.3 %copy-start.6 = (bf16[2048,4]{0,1:T(4,128)(2,1)S(1)}, bf16[2048,4]{0,1:T(4,128)(2,1)}, u32[]{:S(2)}) copy-start(bf16[2048,4]{0,1:T(4,128)(2,1)} %param.24) | copy-start | bytes 49156
  165.9 48.3 %copy-start.5 = (bf16[2048,64]{0,1:T(8,128)(2,1)S(1)}, bf16[2048,64]{0,1:T(8,128)(2,1)}, u32[]{:S(2)}) copy-start(bf16[2048,64]{0,1:T(8,128)(2,1)} %param.25) | copy-start | bytes 786436
  207.6 56.8 %all-to-all-start.1 = ((bf16[64,8,2048]{2,1,0:T(8,128)(2,1)}), bf16[64,8,2048]{2,1,0:T(8,128)(2,1)}, u32[]{:S(2)}, u32[]{:S(2)}) async-start(bf16[64,8,2048]{2,1,0:T(8,128)(2,1)} %fusion), calls=%async_computation.1 | async-start | bytes 4194304 | tf_op jit(solution)/shard_map/all_to_all | solution.py:288
